TPU v7x, 32 devices: a whole 2x2x4 slice. The times are simulated.
32 devices in a mesh: rep: 4 (over z), fs: 4 (over y, x), tp: 2 (over core).
Axes of the slice: x: 2, y: 2, z: 4, core: 2. Of those that a mesh axis runs over, the one named last changes fastest.
Arguments:
- tokens_in: bfloat16 [8192, 2048], P(('rep', 'fs', 'tp')), may hold values from -6 to 6
- norm_gain: float32 [2048], replicated, may hold values from 0.1 to 1.9
- gate_weight: bfloat16 [2048, 3072], P(None, ('fs', 'tp')), may hold values from -0.125 to 0.125
- up_weight: bfloat16 [2048, 3072], P(None, ('fs', 'tp')), may hold values from -0.125 to 0.125
- down_weight: bfloat16 [3072, 2048], P(('fs', 'tp')), may hold values from -0.109375 to 0.109375
- out_grad: bfloat16 [8192, 2048], P(('rep', 'fs', 'tp')), may hold values from -6 to 6
Outputs:
- grad_in: bfloat16 [8192, 2048], P(('rep', 'fs', 'tp'))
- grad_gain: float32 [2048], replicated
- grad_gate: float32 [2048, 3072], P(None, ('fs', 'tp'))
- grad_up: float32 [2048, 3072], P(None, ('fs', 'tp'))
- grad_down: float32 [3072, 2048], P(('fs', 'tp'))
All inputs are finite; a program needn't handle non-finite values.
Results may differ from a plain program's by a relative error of at most 0.014.
Values may be sent and summed in bfloat16 or wider, within the bound.
A program may use at most 192 MiB of HBM per device.

v0:
```python
import jax
import jax.numpy as jnp
from jax import lax
from jax.sharding import PartitionSpec as P

norm_eps = 1e-06


def shards(tokens_in, norm_gain, gate_weight, up_weight, down_weight, out_grad):
    row_count = tokens_in.shape[0]
    total_tokens = row_count * lax.axis_size("rep") * lax.axis_size("fs") * lax.axis_size("tp")
    factor = float(total_tokens) ** (-0.5)
    whole_in, whole_grad = (
        lax.all_gather(tokens_in, ("fs", "tp"), axis=0, tiled=True),
        lax.all_gather(out_grad, ("fs", "tp"), axis=0, tiled=True),
    )
    floats = whole_in.astype(jnp.float32)
    inverse = lax.rsqrt(jnp.mean(floats * floats, axis=-1, keepdims=True) + norm_eps)
    unit_rows = floats * inverse
    normed = (unit_rows * norm_gain).astype(jnp.bfloat16)
    gate_pre = jnp.dot(normed, gate_weight, preferred_element_type=jnp.float32)
    up_pre = jnp.dot(normed, up_weight, preferred_element_type=jnp.float32)
    sigma = jax.nn.sigmoid(gate_pre)
    active = gate_pre * sigma
    hidden = (active * up_pre).astype(jnp.bfloat16)
    grad_hidden = 0.5 * jnp.dot(whole_grad, down_weight.T, preferred_element_type=jnp.float32)
    grad_gate_pre = (grad_hidden * up_pre * sigma * (1.0 + gate_pre * (1.0 - sigma))).astype(
        jnp.bfloat16
    )
    grad_up_pre = (grad_hidden * active).astype(jnp.bfloat16)
    result = jnp.dot(grad_gate_pre, gate_weight.T, preferred_element_type=jnp.float32)
    grad_normed = lax.psum_scatter(
        (result + jnp.dot(grad_up_pre, up_weight.T, preferred_element_type=jnp.float32)).astype(
            jnp.bfloat16
        ),
        ("fs", "tp"),
        scatter_dimension=0,
        tiled=True,
    ).astype(jnp.float32)
    local_gate = jnp.dot(normed.T, grad_gate_pre, preferred_element_type=jnp.float32)
    local_up = jnp.dot(normed.T, grad_up_pre, preferred_element_type=jnp.float32)
    local_down = jnp.dot(hidden.T, whole_grad, preferred_element_type=jnp.float32)
    summed_gate = lax.psum(local_gate.astype(jnp.bfloat16), "rep").astype(jnp.float32)
    summed_up = lax.psum(local_up.astype(jnp.bfloat16), "rep").astype(jnp.float32)
    summed_down = lax.psum(local_down.astype(jnp.bfloat16), "rep").astype(jnp.float32)
    grad_gate = summed_gate * factor
    grad_up = summed_up * factor
    grad_down = summed_down * (0.5 * factor)
    position = lax.axis_index("fs") * lax.axis_size("tp") + lax.axis_index("tp")
    own_unit = lax.dynamic_slice_in_dim(unit_rows, position * row_count, row_count, 0)
    own_inverse = lax.dynamic_slice_in_dim(inverse, position * row_count, row_count, 0)
    gain_local = jnp.sum(grad_normed * own_unit, axis=0)
    gain_partial = lax.psum(gain_local, ("fs", "tp"))
    grad_gain = lax.psum(gain_partial, "rep")
    scaled = grad_normed * norm_gain
    grad_in = (
        out_grad.astype(jnp.float32)
        + own_inverse * scaled
        - own_unit * own_inverse * jnp.mean(scaled * own_unit, axis=-1, keepdims=True)
    )
    return (grad_in.astype(jnp.bfloat16), grad_gain, grad_gate, grad_up, grad_down)


def solution(mesh):
    in_specs = (
        P(("rep", "fs", "tp"), None),
        P(),
        P(None, ("fs", "tp")),
        P(None, ("fs", "tp")),
        P(("fs", "tp"), None),
        P(("rep", "fs", "tp"), None),
    )
    out_specs = (
        P(("rep", "fs", "tp"), None),
        P(),
        P(None, ("fs", "tp")),
        P(None, ("fs", "tp")),
        P(("fs", "tp"), None),
    )
    return jax.shard_map(shards, mesh=mesh, in_specs=in_specs, out_specs=out_specs, check_vma=False)
```

profile of v0, /device:TPU:0, one launch (start us, length us, event | category | flops | bytes accessed | tf_op | source)
XLA Modules:
  0.0 437.0 jit_solution(11326514007255932176)
XLA Ops:
  7.2 0.0 copy-start
  7.2 0.0 all-gather.3.cloned.1.call-start
  7.2 0.0 copy-start.3
  7.2 0.7 all-gather.3.cloned.1.call-update
  7.9 0.0 all-gather.5.cloned.1.call-start
  8.0 0.7 all-gather.5.cloned.1.call-update
  8.7 0.0 copy-start.9
  8.7 0.0 all-reduce.3.cloned.1.call-start
  8.7 58.2 %all-gather.3.cloned.1.call-done = bf16[2048,2048]{1,0:T(8,128)(2,1)} async-done(((bf16[256,2048]{1,0:T(8,128)(2,1)}), bf16[2048,2048]{1,0:T(8,128)(2,1)}) %all-gather.3.cloned.1.call-update) | async-done | bytes 8388624 | tf_op jit(solution)/shard_map/all_gather | solution.py:14
  66.9 5.2 %fusion = f32[2048]{0:T(1024)S(1)} fusion(bf16[2048,2048]{1,0:T(8,128)(2,1)} %all-gather.3.cloned.1.call-done), kind=kLoop, calls=%fused_computation.2 | loop fusion | flops 12580864 | bytes 8396800 | tf_op jit(solution)/shard_map/reduce_sum | solution.py:18
  72.1 0.0 copy-done.3
  72.1 0.0 copy-done.9
  72.2 0.5 copy-done.1
  72.7 6.4 %fusion.12 = f32[2048,384]{1,0:T(8,128)} fusion(bf16[2048,384]{1,0:T(8,128)(2,1)S(1)} %copy-done.3, f32[2048]{0:T(1024)S(1)} %copy-done.9, f32[2048]{0:T(1024)S(1)} %add_rsqrt_fusion, bf16[2048,2048]{1,0:T(8,128)(2,1)S(1)} %copy-done.1), kind=kOutput, calls=%fused_computation.30 | convolution fusion | flops 3238002688 | bytes 13123584 | tf_op jit(solution)/shard_map/dot_general | solution.py:22
  79.0 0.0 copy-done
  79.0 6.3 %fusion.11 = f32[2048,384]{1,0:T(8,128)} fusion(bf16[2048,384]{1,0:T(8,128)(2,1)S(1)} %copy-done, f32[2048]{0:T(1024)S(1)} %copy-done.9, f32[2048]{0:T(1024)S(1)} %add_rsqrt_fusion, bf16[2048,2048]{1,0:T(8,128)(2,1)S(1)} %copy-done.1), kind=kOutput, calls=%fused_computation.29 | convolution fusion | flops 3238002688 | bytes 13123584 | tf_op jit(solution)/shard_map/dot_general | solution.py:21
  85.4 37.7 %all-gather.5.cloned.1.call-done = bf16[2048,2048]{1,0:T(8,128)(2,1)} async-done(((bf16[256,2048]{1,0:T(8,128)(2,1)}), bf16[2048,2048]{1,0:T(8,128)(2,1)}) %all-gather.5.cloned.1.call-update) | async-done | bytes 8388624 | tf_op jit(solution)/shard_map/all_gather | solution.py:15
  123.1 10.3 %convolution_convert_fusion = bf16[384,2048]{1,0:T(8,128)(2,1)} fusion(bf16[2048,2048]{1,0:T(8,128)(2,1)} %all-gather.5.cloned.1.call-done, f32[2048,384]{1,0:T(8,128)} %fusion.12, f32[2048,384]{1,0:T(8,128)} %fusion.11), kind=kOutput, calls=%fused_computation.14 | convolution fusion | flops 3226730496 | bytes 16252928 | tf_op jit(solution)/shard_map/dot_general | solution.py:42
  133.4 0.0 copy-done.10
  133.4 0.0 copy-done.11
  133.4 0.0 copy-done.12
  133.4 0.0 slice-start.1
  133.4 7.5 %multiply_convert_fusion.2 = (bf16[2048,384]{1,0:T(8,128)(2,1)S(1)}, bf16[2048,384]{1,0:T(8,128)(2,1)S(1)}) fusion(f32[2048,384]{1,0:T(8,128)} %fusion.11, f32[2048,384]{1,0:T(8,128)S(1)} %copy-done.12, bf16[2048,2048]{1,0:T(8,128)(2,1)S(1)} %copy-done.10, bf16[384,2048]{1,0:T(8,128)(2,1)S(1)} %copy-done.11), kind=kOutput, calls=%fused_computation.9 | convolution fusion | flops 3232235520 | bytes 19398656 | tf_op jit(solution)/shard_map/dot_general | solution.py:26
  140.9 0.0 copy-start.6
  140.9 0.0 copy-start.8
  140.9 0.0 slice-done
  141.0 0.0 slice-done.1
  141.0 6.1 %convolution_convert_fusion.1 = bf16[2048,384]{1,0:T(8,128)(2,1)} fusion(bf16[2048,384]{1,0:T(8,128)(2,1)S(1)} %get-tuple-element.10, f32[2048]{0:T(1024)S(1)} %copy-done.9, f32[2048]{0:T(1024)S(1)} %add_rsqrt_fusion, bf16[2048,2048]{1,0:T(8,128)(2,1)S(1)} %bitcast.12), kind=kOutput, calls=%fused_computation.15 | convolution fusion | flops 3238789120 | bytes 11550720 | tf_op jit(solution)/shard_map/dot_general | solution.py:41
  147.1 0.0 copy-done.6
  147.1 0.0 copy-done.8
  147.1 6.0 %convolution_convert_fusion.2 = bf16[2048,384]{1,0:T(8,128)(2,1)} fusion(bf16[2048,384]{1,0:T(8,128)(2,1)S(1)} %get-tuple-element.11, f32[2048]{0:T(1024)S(1)} %copy-done.9, f32[2048]{0:T(1024)S(1)} %add_rsqrt_fusion, bf16[2048,2048]{1,0:T(8,128)(2,1)S(1)} %bitcast.12), kind=kOutput, calls=%fused_computation.16 | convolution fusion | flops 3238789120 | bytes 11550720 | tf_op jit(solution)/shard_map/dot_general | solution.py:40
  153.1 0.0 all-reduce.3.cloned.1.call-update
  153.1 0.3 reduce-scatter.2.cloned.1.call-start
  153.4 0.0 copy-start.7
  153.4 10.1 %fusion.13 = f32[2048,2048]{1,0:T(8,128)} fusion(bf16[2048,384]{1,0:T(8,128)(2,1)} %copy-done.8, bf16[2048,384]{1,0:T(8,128)(2,1)S(1)} %copy-done), kind=kOutput, calls=%fused_computation.31 | convolution fusion | flops 3221225472 | bytes 19922944 | tf_op jit(solution)/shard_map/dot_general | solution.py:31
  163.5 0.0 copy-done.7
  163.5 10.3 %add_convert_fusion = bf16[2048,2048]{1,0:T(8,128)(2,1)} fusion(f32[2048,2048]{1,0:T(8,128)} %fusion.13, bf16[2048,384]{1,0:T(8,128)(2,1)S(1)} %copy-done.7, bf16[2048,384]{1,0:T(8,128)(2,1)S(1)} %copy-done.3), kind=kOutput, calls=%fused_computation.3 | convolution fusion | flops 3229614080 | bytes 28311552 | tf_op jit(solution)/shard_map/dot_general | solution.py:33
  173.8 0.0 reduce-scatter.2.cloned.1.call-update
  173.9 0.1 dynamic-slice.3
  174.0 10.4 %convert_multiply_fusion = f32[2048,2048]{1,0:T(8,128)} fusion(bf16[2048,2048]{1,0:T(8,128)(2,1)} %all-gather.3.cloned.1.call-done, f32[2048]{0:T(1024)S(1)} %add_rsqrt_fusion), kind=kLoop, calls=%fused_computation | loop fusion | flops 8388608 | bytes 25174016 | tf_op jit(solution)/shard_map/mul | solution.py:19
  184.3 141.0 %all-reduce.3.cloned.1.call-done = (bf16[2048,384]{1,0:T(8,128)(2,1)}, bf16[2048,384]{1,0:T(8,128)(2,1)}, bf16[384,2048]{1,0:T(8,128)(2,1)}) async-done(((bf16[2048,384]{1,0:T(8,128)(2,1)}, bf16[2048,384]{1,0:T(8,128)(2,1)}, bf16[384,2048]{1,0:T(8,128)(2,1)}), (bf16[2048,384]{1,0:T(8,128)(2,1)}, bf16[2048,384]{1,0:T(8,128)(2,1)}, bf16[384,2048]{1,0:T(8,128)(2,1)})) %all-reduce.3.cloned.1.call-update) | async-done | bytes 4718608 | tf_op jit(solution)/shard_map/psum | solution.py:43
  325.3 3.6 convert_multiply_fusion.2
  328.9 3.3 convert_multiply_fusion.3
  332.2 66.9 %reduce-scatter.2.cloned.1.call-done = bf16[256,2048]{1,0:T(8,128)(2,1)} async-done(((bf16[2048,2048]{1,0:T(8,128)(2,1)}), bf16[256,2048]{1,0:T(8,128)(2,1)}) %reduce-scatter.2.cloned.1.call-update) | async-done | bytes 1048592 | tf_op jit(solution)/shard_map/reduce_scatter | solution.py:32
  399.1 2.6 fusion.8
  401.7 12.8 %psum.35 = f32[2048]{0:T(1024)S(1)} all-reduce(f32[2048]{0:T(1024)S(1)} %get-tuple-element.5), channel_id=1, replica_groups=mesh['rep'=4,'fs'=4,'tp'=2] {'fs','tp'}, use_global_device_ids=true, to_apply=%region_4.0 | all-reduce | flops 2048 | bytes 16384 | tf_op jit(solution)/shard_map/psum | solution.py:53
  414.4 12.4 %psum.36 = f32[2048]{0:T(1024)} all-reduce(f32[2048]{0:T(1024)S(1)} %psum.35), channel_id=1, replica_groups=mesh['rep'=4,'fs'=4,'tp'=2] {'rep'}, use_global_device_ids=true, to_apply=%region_5.0 | all-reduce | flops 2048 | bytes 16384 | tf_op jit(solution)/shard_map/psum | solution.py:54
  426.9 3.6 fusion.6
  (14 shorter events, 0.0 us)
Async XLA Ops:
  7.2 71.8 %copy-start = (bf16[2048,384]{1,0:T(8,128)(2,1)S(1)}, bf16[2048,384]{1,0:T(8,128)(2,1)}, u32[]{:S(2)}) copy-start(bf16[2048,384]{1,0:T(8,128)(2,1)} %param.8) | copy-start | bytes 4718596
  7.2 59.7 %all-gather.3.cloned.1.call-start = ((), (), s32[]{:S(2)}) async-start(), calls=%async_computation.1 | async-start | bytes 9437184 | tf_op jit(solution)/shard_map/all_gather | solution.py:14
  7.2 64.9 %copy-start.3 = (bf16[2048,384]{1,0:T(8,128)(2,1)S(1)}, bf16[2048,384]{1,0:T(8,128)(2,1)}, u32[]{:S(2)}) copy-start(bf16[2048,384]{1,0:T(8,128)(2,1)} %param.9) | copy-start | bytes 4718596
  7.9 115.2 %all-gather.5.cloned.1.call-start = ((), (), s32[]{:S(2)}) async-start(), calls=%async_computation.2 | async-start | bytes 9437184 | tf_op jit(solution)/shard_map/all_gather | solution.py:15
  8.7 63.5 %copy-start.9 = (f32[2048]{0:T(1024)S(1)}, f32[2048]{0:T(1024)}, u32[]{:S(2)}) copy-start(f32[2048]{0:T(1024)} %param.7) | copy-start | bytes 24580
  8.7 316.6 %all-reduce.3.cloned.1.call-start = ((), (), s32[]{:S(2)}) async-start(), calls=%async_computation.4 | async-start | bytes 9437184 | tf_op jit(solution)/shard_map/psum | solution.py:43
  66.9 5.8 %copy-start.1 = (bf16[2048,2048]{1,0:T(8,128)(2,1)S(1)}, bf16[2048,2048]{1,0:T(8,128)(2,1)}, u32[]{:S(2)}) copy-start(bf16[2048,2048]{1,0:T(8,128)(2,1)} %all-gather.3.cloned.1.call-done) | copy-start | bytes 25165828
  123.1 10.4 %copy-start.10 = (bf16[2048,2048]{1,0:T(8,128)(2,1)S(1)}, bf16[2048,2048]{1,0:T(8,128)(2,1)}, u32[]{:S(2)}) copy-start(bf16[2048,2048]{1,0:T(8,128)(2,1)} %all-gather.5.cloned.1.call-done) | copy-start | bytes 25165828
  123.1 10.4 %copy-start.11 = (bf16[384,2048]{1,0:T(8,128)(2,1)S(1)}, bf16[384,2048]{1,0:T(8,128)(2,1)}, u32[]{:S(2)}) copy-start(bf16[384,2048]{1,0:T(8,128)(2,1)} %param.10) | copy-start | bytes 4718596
  123.1 10.4 %copy-start.12 = (f32[2048,384]{1,0:T(8,128)S(1)}, f32[2048,384]{1,0:T(8,128)}, u32[]{:S(2)}) copy-start(f32[2048,384]{1,0:T(8,128)} %fusion.12) | copy-start | bytes 9437188
  123.1 17.9 %slice-start = ((s8[8388608]{0:T(1024)(128)(4,1)}), s8[4194304]{0:T(1024)(128)(4,1)S(1)}, s32[]{:S(2)}) async-start(s8[8388608]{0:T(1024)(128)(4,1)} %bitcast.11), calls=%async_computation.5 | async-start | bytes 8388608
  133.4 7.5 %slice-start.1 = ((s8[8388608]{0:T(1024)(128)(4,1)}), s8[4194304]{0:T(1024)(128)(4,1)S(1)}, s32[]{:S(2)}) async-start(s8[8388608]{0:T(1024)(128)(4,1)} %bitcast.11), calls=%async_computation.6 | async-start | bytes 8388608
  140.9 6.1 %copy-start.6 = (bf16[2048,384]{1,0:T(8,128)(2,1)}, bf16[2048,384]{1,0:T(8,128)(2,1)S(1)}, u32[]{:S(2)}) copy-start(bf16[2048,384]{1,0:T(8,128)(2,1)S(1)} %get-tuple-element.10) | copy-start | bytes 4718596
  140.9 6.1 %copy-start.8 = (bf16[2048,384]{1,0:T(8,128)(2,1)}, bf16[2048,384]{1,0:T(8,128)(2,1)S(1)}, u32[]{:S(2)}) copy-start(bf16[2048,384]{1,0:T(8,128)(2,1)S(1)} %get-tuple-element.11) | copy-start | bytes 4718596
  153.1 246.0 %reduce-scatter.2.cloned.1.call-start = ((), (), s32[]{:S(2)}) async-start(), calls=%async_computation.3 | async-start | bytes 9437184 | tf_op jit(solution)/shard_map/reduce_scatter | solution.py:32
  153.4 10.1 %copy-start.7 = (bf16[2048,384]{1,0:T(8,128)(2,1)S(1)}, bf16[2048,384]{1,0:T(8,128)(2,1)}, u32[]{:S(2)}) copy-start(bf16[2048,384]{1,0:T(8,128)(2,1)} %copy-done.6) | copy-start | bytes 4718596
  325.3 3.6 copy-start.4
  325.3 3.6 copy-start.5
  332.2 94.7 %copy-start.2 = (bf16[256,2048]{1,0:T(8,128)(2,1)S(1)}, bf16[256,2048]{1,0:T(8,128)(2,1)}, u32[]{:S(2)}) copy-start(bf16[256,2048]{1,0:T(8,128)(2,1)} %param.11) | copy-start | bytes 3145732
Sparse Core Ops, SparseCore 0:
  9.9 56.9 all-gather.2
  68.8 54.2 all-gather.4
  153.3 171.9 all-reduce.2
  328.6 70.4 reduce-scatter.1
where the time goes:
time: 437 us
  waiting for transfers between devices  305 us (70%)
  matrix products  63.1 us (14%)
  other arithmetic  28.6 us (7%)
  blocking collectives  25.2 us (6%)
  between operations  13.9 us (3%)
    psum x1, waiting for transfers between devices, shards(): lax.psum(local_gate.astype(jnp.bfloat16), 'rep').astype(jnp.float32)  141 us
    reduce_scatter x1, waiting for transfers between devices, shards(): lax.psum_scatter((result + jnp.dot(grad_up_pre, up_weight.T, preferred_el...  66.9 us
    all_gather x1, waiting for transfers between devices, shards(): lax.all_gather(tokens_in, ('fs', 'tp'), axis=0, tiled=True)  58.2 us
    all_gather x1, waiting for transfers between devices, shards(): lax.all_gather(out_grad, ('fs', 'tp'), axis=0, tiled=True)  37.7 us
    psum x1, blocking collectives, shards(): gain_partial = lax.psum(gain_local, ('fs', 'tp'))  12.8 us
    psum x1, blocking collectives, shards(): grad_gain = lax.psum(gain_partial, 'rep')  12.4 us
    mul x1, other arithmetic, shards(): unit_rows = floats * inverse  10.4 us
    dot_general x1, matrix products, shards(): jnp.dot(hidden.T, whole_grad, preferred_element_type=jnp.float32)  10.3 us
  transfers between devices with their start and end apart: 4, of which 4 were waited for; matrix products, arithmetic and copies ran while one was open for 13% of the time, Pallas kernels for 0%

commit v1 on v0

--- a/solution.py
+++ b/solution.py
@@ -4,6 +4,12 @@
 from jax.sharding import PartitionSpec as P
 
 norm_eps = 1e-06
+
+
+def arrange_goods(field_in, across):
+    b_now = lax.all_gather(field_in, axis_name=across)
+    h_now = jnp.sum(b_now, axis=0)
+    return h_now
 
 
 def shards(tokens_in, norm_gain, gate_weight, up_weight, down_weight, out_grad):
@@ -40,7 +46,7 @@
     local_gate = jnp.dot(normed.T, grad_gate_pre, preferred_element_type=jnp.float32)
     local_up = jnp.dot(normed.T, grad_up_pre, preferred_element_type=jnp.float32)
     local_down = jnp.dot(hidden.T, whole_grad, preferred_element_type=jnp.float32)
-    summed_gate = lax.psum(local_gate.astype(jnp.bfloat16), "rep").astype(jnp.float32)
+    summed_gate = arrange_goods(local_gate.astype(jnp.bfloat16), "rep").astype(jnp.float32)
     summed_up = lax.psum(local_up.astype(jnp.bfloat16), "rep").astype(jnp.float32)
     summed_down = lax.psum(local_down.astype(jnp.bfloat16), "rep").astype(jnp.float32)
     grad_gate = summed_gate * factor

time: 437 us -> 498 us (1.14)
  waiting for transfers between devices: 305 us -> 355 us
  other arithmetic: 28.6 us -> 33.9 us
    all_gather x0 -> x1, waiting for transfers between devices: none -> 111 us  [arrange_goods(): b_now = lax.all_gather(field_in, axis_name=across)]
    psum x1, waiting for transfers between devices: 141 us -> 80.3 us  [shards(): lax.psum(local_up.astype(jnp.bfloat16), 'rep').astype(jnp.float32)]
  transfers between devices with their start and end apart: 4 -> 5, of which waited for: 4 -> 5; matrix products, arithmetic and copies ran while one was open for 13% -> 14% of each run, Pallas kernels for 0% -> 0%
where the time goes in v1:
time: 498 us
  waiting for transfers between devices  355 us (71%)
  matrix products  67.5 us (14%)
  other arithmetic  33.9 us (7%)
  blocking collectives  25.2 us (5%)
  between operations  13.9 us (3%)
    all_gather x1, waiting for transfers between devices, arrange_goods(): b_now = lax.all_gather(field_in, axis_name=across)  111 us
    psum x1, waiting for transfers between devices, shards(): lax.psum(local_up.astype(jnp.bfloat16), 'rep').astype(jnp.float32)  80.3 us
    reduce_scatter x1, waiting for transfers between devices, shards(): lax.psum_scatter((result + jnp.dot(grad_up_pre, up_weight.T, preferred_el...  66.3 us
    all_gather x1, waiting for transfers between devices, shards(): lax.all_gather(tokens_in, ('fs', 'tp'), axis=0, tiled=True)  58.2 us
    all_gather x1, waiting for transfers between devices, shards(): lax.all_gather(out_grad, ('fs', 'tp'), axis=0, tiled=True)  37.7 us
    psum x1, blocking collectives, shards(): gain_partial = lax.psum(gain_local, ('fs', 'tp'))  12.8 us
    psum x1, blocking collectives, shards(): grad_gain = lax.psum(gain_partial, 'rep')  12.4 us
    dot_general x1, matrix products, shards(): jnp.dot(grad_up_pre, up_weight.T, preferred_element_type=jnp.float32)  10.4 us
  transfers between devices with their start and end apart: 5, of which 5 were waited for; matrix products, arithmetic and copies ran while one was open for 14% of the time, Pallas kernels for 0%

profile of v1, /device:TPU:0, one launch (start us, length us, event | category | flops | bytes accessed | tf_op | source)
XLA Modules:
  0.0 497.5 jit_solution(1765138514429238805)
XLA Ops:
  7.2 0.0 copy-start
  7.2 0.0 all-gather.5.cloned.1.call-start
  7.2 0.0 copy-start.3
  7.2 0.7 all-gather.5.cloned.1.call-update
  7.9 0.0 all-gather.7.cloned.1.call-start
  8.0 0.7 all-gather.7.cloned.1.call-update
  8.7 0.0 copy-start.7
  8.7 0.0 all-reduce.3.cloned.1.call-start
  8.7 58.2 %all-gather.5.cloned.1.call-done = bf16[2048,2048]{1,0:T(8,128)(2,1)} async-done(((bf16[256,2048]{1,0:T(8,128)(2,1)}), bf16[2048,2048]{1,0:T(8,128)(2,1)}) %all-gather.5.cloned.1.call-update) | async-done | bytes 8388624 | tf_op jit(solution)/shard_map/all_gather | solution.py:20
  66.9 5.2 %fusion = f32[2048]{0:T(1024)S(1)} fusion(bf16[2048,2048]{1,0:T(8,128)(2,1)} %all-gather.5.cloned.1.call-done), kind=kLoop, calls=%fused_computation.2 | loop fusion | flops 12580864 | bytes 8396800 | tf_op jit(solution)/shard_map/reduce_sum | solution.py:24
  72.1 0.0 copy-done.3
  72.1 0.0 copy-done.7
  72.2 0.5 copy-done.1
  72.7 6.4 %fusion.12 = f32[2048,384]{1,0:T(8,128)} fusion(bf16[2048,384]{1,0:T(8,128)(2,1)S(1)} %copy-done.3, f32[2048]{0:T(1024)S(1)} %copy-done.7, f32[2048]{0:T(1024)S(1)} %add_rsqrt_fusion, bf16[2048,2048]{1,0:T(8,128)(2,1)S(1)} %copy-done.1), kind=kOutput, calls=%fused_computation.30 | convolution fusion | flops 3238002688 | bytes 13123584 | tf_op jit(solution)/shard_map/dot_general | solution.py:28
  79.0 0.0 copy-done
  79.0 6.3 %fusion.11 = f32[2048,384]{1,0:T(8,128)} fusion(bf16[2048,384]{1,0:T(8,128)(2,1)S(1)} %copy-done, f32[2048]{0:T(1024)S(1)} %copy-done.7, f32[2048]{0:T(1024)S(1)} %add_rsqrt_fusion, bf16[2048,2048]{1,0:T(8,128)(2,1)S(1)} %copy-done.1), kind=kOutput, calls=%fused_computation.29 | convolution fusion | flops 3238002688 | bytes 13123584 | tf_op jit(solution)/shard_map/dot_general | solution.py:27
  85.4 37.7 %all-gather.7.cloned.1.call-done = bf16[2048,2048]{1,0:T(8,128)(2,1)} async-done(((bf16[256,2048]{1,0:T(8,128)(2,1)}), bf16[2048,2048]{1,0:T(8,128)(2,1)}) %all-gather.7.cloned.1.call-update) | async-done | bytes 8388624 | tf_op jit(solution)/shard_map/all_gather | solution.py:21
  123.1 10.3 %convolution_convert_fusion = bf16[384,2048]{1,0:T(8,128)(2,1)} fusion(bf16[2048,2048]{1,0:T(8,128)(2,1)} %all-gather.7.cloned.1.call-done, f32[2048,384]{1,0:T(8,128)} %fusion.12, f32[2048,384]{1,0:T(8,128)} %fusion.11), kind=kOutput, calls=%fused_computation.14 | convolution fusion | flops 3226730496 | bytes 16252928 | tf_op jit(solution)/shard_map/dot_general | solution.py:48
  133.4 0.0 copy-done.8
  133.4 0.0 copy-done.9
  133.4 0.0 copy-done.10
  133.4 0.0 slice-start.1
  133.4 8.3 %multiply_convert_fusion.2 = (bf16[2048,384]{1,0:T(8,128)(2,1)S(1)}, bf16[2048,384]{1,0:T(8,128)(2,1)}) fusion(f32[2048,384]{1,0:T(8,128)} %fusion.11, f32[2048,384]{1,0:T(8,128)S(1)} %copy-done.10, bf16[2048,2048]{1,0:T(8,128)(2,1)S(1)} %copy-done.8, bf16[384,2048]{1,0:T(8,128)(2,1)S(1)} %copy-done.9), kind=kOutput, calls=%fused_computation.9 | convolution fusion | flops 3232235520 | bytes 19398656 | tf_op jit(solution)/shard_map/dot_general | solution.py:32
  141.8 1.1 copy-done.4
  142.9 6.1 %convolution_convert_fusion.1 = bf16[2048,384]{1,0:T(8,128)(2,1)} fusion(bf16[2048,384]{1,0:T(8,128)(2,1)S(1)} %get-tuple-element.9, f32[2048]{0:T(1024)S(1)} %copy-done.7, f32[2048]{0:T(1024)S(1)} %add_rsqrt_fusion, bf16[2048,2048]{1,0:T(8,128)(2,1)S(1)} %bitcast.13), kind=kOutput, calls=%fused_computation.15 | convolution fusion | flops 3238789120 | bytes 11550720 | tf_op jit(solution)/shard_map/dot_general | solution.py:47
  149.0 0.0 all-reduce.3.cloned.1.call-update
  149.0 0.0 all-gather.9.cloned.1.call-start
  149.1 9.9 %convolution_convert_fusion.2 = bf16[2048,384]{1,0:T(8,128)(2,1)} fusion(bf16[2048,384]{1,0:T(8,128)(2,1)} %get-tuple-element.10, f32[2048]{0:T(1024)S(1)} %copy-done.7, f32[2048]{0:T(1024)S(1)} %add_rsqrt_fusion, bf16[2048,2048]{1,0:T(8,128)(2,1)} %all-gather.5.cloned.1.call-done), kind=kOutput, calls=%fused_computation.16 | convolution fusion | flops 3238789120 | bytes 11550720 | tf_op jit(solution)/shard_map/dot_general | solution.py:46
  159.0 0.0 all-gather.9.cloned.1.call-update
  159.0 0.3 reduce-scatter.2.cloned.1.call-start
  159.3 0.0 copy-start.5
  159.3 9.8 %fusion.13 = f32[2048,2048]{1,0:T(8,128)} fusion(bf16[2048,384]{1,0:T(8,128)(2,1)} %get-tuple-element.10, bf16[2048,384]{1,0:T(8,128)(2,1)S(1)} %copy-done), kind=kOutput, calls=%fused_computation.31 | convolution fusion | flops 3221225472 | bytes 19922944 | tf_op jit(solution)/shard_map/dot_general | solution.py:37
  169.1 0.0 copy-done.5
  169.1 10.4 %add_convert_fusion = bf16[2048,2048]{1,0:T(8,128)(2,1)} fusion(f32[2048,2048]{1,0:T(8,128)} %fusion.13, bf16[2048,384]{1,0:T(8,128)(2,1)S(1)} %copy-done.5, bf16[2048,384]{1,0:T(8,128)(2,1)S(1)} %copy-done.3), kind=kOutput, calls=%fused_computation.3 | convolution fusion | flops 3229614080 | bytes 28311552 | tf_op jit(solution)/shard_map/dot_general | solution.py:39
  179.5 0.0 reduce-scatter.2.cloned.1.call-update
  179.5 0.1 dynamic-slice.3
  179.6 10.4 %convert_multiply_fusion = f32[2048,2048]{1,0:T(8,128)} fusion(bf16[2048,2048]{1,0:T(8,128)(2,1)} %all-gather.5.cloned.1.call-done, f32[2048]{0:T(1024)S(1)} %add_rsqrt_fusion), kind=kLoop, calls=%fused_computation | loop fusion | flops 8388608 | bytes 25174016 | tf_op jit(solution)/shard_map/mul | solution.py:25
  189.9 80.3 %all-reduce.3.cloned.1.call-done = (bf16[2048,384]{1,0:T(8,128)(2,1)}, bf16[384,2048]{1,0:T(8,128)(2,1)}) async-done(((bf16[2048,384]{1,0:T(8,128)(2,1)}, bf16[384,2048]{1,0:T(8,128)(2,1)}), (bf16[2048,384]{1,0:T(8,128)(2,1)}, bf16[384,2048]{1,0:T(8,128)(2,1)})) %all-reduce.3.cloned.1.call-update) | async-done | bytes 3145744 | tf_op jit(solution)/shard_map/psum | solution.py:50
  270.3 3.6 convert_multiply_fusion.2
  273.8 1.9 convert_multiply_fusion.3
  275.8 110.8 %all-gather.9.cloned.1.call-done = bf16[8192,384]{1,0:T(8,128)(2,1)} async-done(((bf16[2048,384]{1,0:T(8,128)(2,1)}), bf16[8192,384]{1,0:T(8,128)(2,1)}) %all-gather.9.cloned.1.call-update) | async-done | bytes 6291472 | tf_op jit(solution)/shard_map/all_gather | solution.py:10
  386.6 4.7 reduce_sum.42
  391.4 1.9 convert_multiply_fusion.4
  393.3 66.3 %reduce-scatter.2.cloned.1.call-done = bf16[256,2048]{1,0:T(8,128)(2,1)} async-done(((bf16[2048,2048]{1,0:T(8,128)(2,1)}), bf16[256,2048]{1,0:T(8,128)(2,1)}) %reduce-scatter.2.cloned.1.call-update) | async-done | bytes 1048592 | tf_op jit(solution)/shard_map/reduce_scatter | solution.py:38
  459.7 2.6 fusion.8
  462.2 12.8 %psum.28 = f32[2048]{0:T(1024)S(1)} all-reduce(f32[2048]{0:T(1024)S(1)} %get-tuple-element.5), channel_id=1, replica_groups=mesh['rep'=4,'fs'=4,'tp'=2] {'fs','tp'}, use_global_device_ids=true, to_apply=%region_4.0 | all-reduce | flops 2048 | bytes 16384 | tf_op jit(solution)/shard_map/psum | solution.py:59
  475.0 12.4 %psum.29 = f32[2048]{0:T(1024)} all-reduce(f32[2048]{0:T(1024)S(1)} %psum.28), channel_id=1, replica_groups=mesh['rep'=4,'fs'=4,'tp'=2] {'rep'}, use_global_device_ids=true, to_apply=%region_5.0 | all-reduce | flops 2048 | bytes 16384 | tf_op jit(solution)/shard_map/psum | solution.py:60
  487.4 3.6 fusion.6
  (15 shorter events, 0.0 us)
Async XLA Ops:
  7.2 71.8 %copy-start = (bf16[2048,384]{1,0:T(8,128)(2,1)S(1)}, bf16[2048,384]{1,0:T(8,128)(2,1)}, u32[]{:S(2)}) copy-start(bf16[2048,384]{1,0:T(8,128)(2,1)} %param.8) | copy-start | bytes 4718596
  7.2 59.7 %all-gather.5.cloned.1.call-start = ((), (), s32[]{:S(2)}) async-start(), calls=%async_computation.1 | async-start | bytes 9437184 | tf_op jit(solution)/shard_map/all_gather | solution.py:20
  7.2 64.9 %copy-start.3 = (bf16[2048,384]{1,0:T(8,128)(2,1)S(1)}, bf16[2048,384]{1,0:T(8,128)(2,1)}, u32[]{:S(2)}) copy-start(bf16[2048,384]{1,0:T(8,128)(2,1)} %param.9) | copy-start | bytes 4718596
  7.9 115.2 %all-gather.7.cloned.1.call-start = ((), (), s32[]{:S(2)}) async-start(), calls=%async_computation.2 | async-start | bytes 9437184 | tf_op jit(solution)/shard_map/all_gather | solution.py:21
  8.7 63.5 %copy-start.7 = (f32[2048]{0:T(1024)S(1)}, f32[2048]{0:T(1024)}, u32[]{:S(2)}) copy-start(f32[2048]{0:T(1024)} %param.7) | copy-start | bytes 24580
  8.7 261.6 %all-reduce.3.cloned.1.call-start = ((), (), s32[]{:S(2)}) async-start(), calls=%async_computation.5 | async-start | bytes 6291456 | tf_op jit(solution)/shard_map/psum | solution.py:50
  66.9 5.8 %copy-start.1 = (bf16[2048,2048]{1,0:T(8,128)(2,1)S(1)}, bf16[2048,2048]{1,0:T(8,128)(2,1)}, u32[]{:S(2)}) copy-start(bf16[2048,2048]{1,0:T(8,128)(2,1)} %all-gather.5.cloned.1.call-done) | copy-start | bytes 25165828
  123.1 10.3 %copy-start.8 = (bf16[2048,2048]{1,0:T(8,128)(2,1)S(1)}, bf16[2048,2048]{1,0:T(8,128)(2,1)}, u32[]{:S(2)}) copy-start(bf16[2048,2048]{1,0:T(8,128)(2,1)} %all-gather.7.cloned.1.call-done) | copy-start | bytes 25165828
  123.1 10.3 %copy-start.9 = (bf16[384,2048]{1,0:T(8,128)(2,1)S(1)}, bf16[384,2048]{1,0:T(8,128)(2,1)}, u32[]{:S(2)}) copy-start(bf16[384,2048]{1,0:T(8,128)(2,1)} %param.10) | copy-start | bytes 4718596
  123.1 10.4 %copy-start.10 = (f32[2048,384]{1,0:T(8,128)S(1)}, f32[2048,384]{1,0:T(8,128)}, u32[]{:S(2)}) copy-start(f32[2048,384]{1,0:T(8,128)} %fusion.12) | copy-start | bytes 9437188
  123.1 19.8 %slice-start = ((s8[8388608]{0:T(1024)(128)(4,1)}), s8[4194304]{0:T(1024)(128)(4,1)S(1)}, s32[]{:S(2)}) async-start(s8[8388608]{0:T(1024)(128)(4,1)} %bitcast.12), calls=%async_computation.6 | async-start | bytes 8388608
  133.4 9.5 %slice-start.1 = ((s8[8388608]{0:T(1024)(128)(4,1)}), s8[4194304]{0:T(1024)(128)(4,1)S(1)}, s32[]{:S(2)}) async-start(s8[8388608]{0:T(1024)(128)(4,1)} %bitcast.12), calls=%async_computation.7 | async-start | bytes 8388608
  141.8 1.1 copy-start.4
  149.0 237.6 %all-gather.9.cloned.1.call-start = ((), (), s32[]{:S(2)}) async-start(), calls=%async_computation.4 | async-start | bytes 7864320 | tf_op jit(solution)/shard_map/all_gather | solution.py:10
  159.0 300.6 %reduce-scatter.2.cloned.1.call-start = ((), (), s32[]{:S(2)}) async-start(), calls=%async_computation.3 | async-start | bytes 9437184 | tf_op jit(solution)/shard_map/reduce_scatter | solution.py:38
  159.3 9.8 %copy-start.5 = (bf16[2048,384]{1,0:T(8,128)(2,1)S(1)}, bf16[2048,384]{1,0:T(8,128)(2,1)}, u32[]{:S(2)}) copy-start(bf16[2048,384]{1,0:T(8,128)(2,1)} %copy-done.4) | copy-start | bytes 4718596
  270.3 3.6 copy-start.6
  393.3 94.1 %copy-start.2 = (bf16[256,2048]{1,0:T(8,128)(2,1)S(1)}, bf16[256,2048]{1,0:T(8,128)(2,1)}, u32[]{:S(2)}) copy-start(bf16[256,2048]{1,0:T(8,128)(2,1)} %param.11) | copy-start | bytes 3145732
Sparse Core Ops, SparseCore 0:
  9.9 56.9 all-gather.4
  68.8 54.2 all-gather.6
  149.1 121.0 all-reduce.2
  272.3 114.3 all-gather.8
  389.9 69.6 reduce-scatter.1
